TPU v7x, 512 devices: a whole 4x8x8 slice. The times are simulated.
512 devices in a mesh: sp: 32 (over z, x), tp: 16 (over y, core).
Axes of the slice: x: 4, y: 8, z: 8, core: 2. Of those that a mesh axis runs over, the one named last changes fastest.
Arguments:
- skip_stream_entering: bfloat16 [4096, 2048], P('sp', 'tp'), may hold values from -24 to 24
- unfiltered_channel_feed: bfloat16 [4096, 2048], P('sp', 'tp'), may hold values from -6 to 6
- unfiltered_state_entry: bfloat16 [4096, 2048], P('sp', 'tp'), may hold values from -6 to 6
- unfiltered_state_exit: bfloat16 [4096, 2048], P('sp', 'tp'), may hold values from -6 to 6
- final_valve_preactivation: bfloat16 [4096, 2048], P('sp', 'tp'), may hold values from -6 to 6
- increment_preactivation: float32 [2, 32, 4096], P(None, 'tp', 'sp'), may hold values from -8 to 8
- summed_attenuation_both_ways: float32 [2, 32, 4096], P(None, 'tp', 'sp'), may hold values from -0.7 to 0, as said below
- channel_fading_speed: float32 [2, 32], P(None, 'tp'), may hold values from 4.8828125e-05 to 0.03, as said below
- channel_feed_filter: float32 [5, 2048], P(None, 'tp'), may hold values from -2.5 to 2.5
- state_entry_filter: float32 [5, 2048], P(None, 'tp'), may hold values from -2.5 to 2.5
- state_exit_filter: float32 [5, 2048], P(None, 'tp'), may hold values from -2.5 to 2.5
- clustered_rescale_factor: float32 [2048], P('tp'), may hold values from 0.1 to 1.9
- final_projection_weights: bfloat16 [2048, 2048], P(None, 'tp'), may hold values from -0.125 to 0.125
- specialist_rescale_factor: float32 [2048], replicated, may hold values from 0.1 to 1.9
- item_specialist_couple: int32 [4096, 2], P('sp'), may hold values from 0 to 31, all different within a row; in each aligned block of 128 rows (0 to 127, 128 to 255, ...) at most 16 rows name the same one
- selected_cluster_likelihood: float32 [4096], P('sp'), may hold values from 0.3 to 1
- selected_twin_scores_raw: float32 [4096, 2], P('sp'), may hold values from -6 to 6
- specialist_gating_weights: bfloat16 [32, 2048, 4096], P('sp', None, 'tp'), may hold values from -0.125 to 0.125
- specialist_raising_weights: bfloat16 [32, 2048, 4096], P('sp', None, 'tp'), may hold values from -0.125 to 0.125
- specialist_lowering_weights: bfloat16 [32, 4096, 2048], P('sp', 'tp'), may hold values from -0.09375 to 0.09375
Outputs:
- layer_out: bfloat16 [4096, 2048], P('sp', 'tp')
Inputs may be any that keep to these rules, and one draw needn't show every extreme that they name: For every head, dt times channel_fading_speed at the rate of the draw sets how far a state is carried; summed_attenuation_both_ways holds a few sharp losses of state. `summed_attenuation_both_ways`: mostly zero. `item_specialist_couple`: the two experts of a row differ. Among the rows of one index of sp (aligned blocks of 128 rows) no expert is named by more than 16 rows, a bound that some expert reaches in some blocks.
All inputs are finite; a program needn't handle non-finite values.
Results may differ from a plain program's by a relative error of at most 0.0095.
Values may be sent and summed in bfloat16 or wider, within the bound.
No kernel may reach another device: no remote copies, remote signals or barrier semaphores. Data moves between devices by JAX's collectives and lax.ppermute only.
A program may use at most 64 MiB of HBM per device.

v0:
```python
import jax
import jax.numpy as jnp
from jax import lax
from jax.sharding import Mesh
from jax.sharding import PartitionSpec as P

D = 2048
HD = 64
NS = 128
CONV = 5
SP = ("sp_0", "sp_1")
HIGHEST = lax.Precision.HIGHEST
group_eps = 1e-05
stream_eps = 1e-06


def extended(cells, sides, width):
    for axis, dim in sides:
        count = lax.axis_size(axis)
        ends = count - 1
        head = lax.slice_in_dim(cells, 0, width, axis=dim)
        tail = lax.slice_in_dim(cells, cells.shape[dim] - width, cells.shape[dim], axis=dim)
        cells = jnp.concatenate(
            [
                lax.ppermute(tail, axis, [(i, (i + 1) % count) for i in range(ends)]),
                cells,
                lax.ppermute(head, axis, [((i + 1) % count, i) for i in range(ends)]),
            ],
            axis=dim,
        )
    return cells


def filled_with(shard, identity):
    return jax.tree.map(
        lambda a, e: jnp.broadcast_to(jnp.asarray(e, a.dtype), a.shape), shard, identity
    )


def all_in_one(shard, axis):
    leaves = jax.tree.leaves(shard)
    sequence = sorted(range(len(leaves)), key=lambda k: -leaves[k].size)
    width = (1, *leaves[sequence[0]].shape)[-1]
    lines = [
        jnp.pad(leaves[k].reshape(-1), (0, -leaves[k].size % width)).reshape(-1, width)
        for k in sequence
    ]
    both, at, found = (lax.all_gather(jnp.concatenate(lines), axis), 0, {})
    for k, line in zip(sequence, lines):
        share = both[:, at : at + len(line)].reshape(len(both), -1)
        found[k] = share[:, : leaves[k].size].reshape(-1, *leaves[k].shape)
        at += len(line)
    numbers = iter(range(len(leaves)))
    return jax.tree.map(lambda _: found[next(numbers)], shard)


def carried_in(shard, axes, combine, identity, reverse):
    before = start = filled_with(shard, identity)
    so_far = shard
    for axis in reversed(axes):
        peers, mine = (lax.axis_size(axis), lax.axis_index(axis))
        pieces = all_in_one(
            jax.tree.map(
                lambda part, kind: part.astype(kind), so_far, (jnp.bfloat16, jnp.bfloat16)
            ),
            axis,
        )
        inside, so_far = (start, start)
        for k in reversed(range(peers)) if reverse else range(peers):
            passed = k > mine if reverse else k < mine
            so_far = combine(
                so_far, jax.tree.map(lambda part, own: part[k].astype(own.dtype), pieces, shard)
            )
            inside = jax.tree.map(lambda new, old: jnp.where(passed, new, old), so_far, inside)
        before = combine(inside, before)
    return before


def in_blocks(shard, dim, peers):
    shape = shard.shape
    parts = shard.reshape(*shape[:dim], peers, shape[dim] // peers, *shape[dim + 1 :])
    return jnp.moveaxis(parts, dim, 0)


def sum_at_owner(shard, axis, dim):
    peers = lax.axis_size(axis)
    parts = lax.all_to_all(in_blocks(shard, dim, peers), axis, 0, 0, tiled=True)
    return jnp.sum(parts.astype(jnp.float32), axis=0)


def block_parts(x_short, b_short, c_short, step_f, step_b, log_f, log_b):
    head_count = x_short.shape[1]
    group_count = b_short.shape[1]
    per_group = head_count // group_count
    length = x_short.shape[0]
    group_scores = jnp.einsum("tgn,sgn->gts", c_short, b_short, preferred_element_type=jnp.float32)
    x_block = x_short.astype(jnp.float32)
    b_block = b_short.astype(jnp.float32)
    c_block = c_short.astype(jnp.float32)
    scores = jnp.repeat(group_scores, per_group, axis=0)
    b_head = jnp.repeat(b_block, per_group, axis=1)
    c_head = jnp.repeat(c_block, per_group, axis=1)
    forward = jnp.cumsum(log_f, axis=1)
    backward = jnp.flip(jnp.cumsum(jnp.flip(log_b, 1), axis=1), 1)
    row_index = lax.broadcasted_iota(jnp.int32, (length, length), 0)
    col_index = lax.broadcasted_iota(jnp.int32, (length, length), 1)
    lower_mask = (col_index <= row_index)[None]
    upper_mask = (col_index >= row_index)[None]
    decay_fwd = jnp.where(
        lower_mask, jnp.exp(jnp.minimum(forward[:, :, None] - forward[:, None, :], 0.0)), 0.0
    )
    decay_bwd = jnp.where(
        upper_mask, jnp.exp(jnp.minimum(backward[:, :, None] - backward[:, None, :], 0.0)), 0.0
    )
    mixing = scores * (decay_fwd * step_f[:, None, :] + decay_bwd * step_b[:, None, :])
    within = jnp.einsum("hts,shp->thp", mixing, x_block, precision=HIGHEST)
    weight_fwd = jnp.exp(forward[:, -1:] - forward) * step_f
    weight_bwd = jnp.exp(backward[:, :1] - backward) * step_b
    state_fwd = jnp.einsum("hs,shp,shn->hpn", weight_fwd, x_block, b_head, precision=HIGHEST)
    state_bwd = jnp.einsum("hs,shp,shn->hpn", weight_bwd, x_block, b_head, precision=HIGHEST)
    return (
        within,
        state_fwd,
        state_bwd,
        forward[:, -1],
        backward[:, 0],
        jnp.exp(forward),
        jnp.exp(backward),
        c_head,
    )


def read_state(c_head, factor, state):
    return (
        jnp.einsum("thn,hpn->thp", c_head, state, precision=HIGHEST)
        * jnp.transpose(factor)[:, :, None]
    )


def compose(earlier, later):
    return (earlier[0] + later[0], earlier[1] * jnp.exp(later[0])[:, None, None] + later[1])


def body(
    skip_stream_entering,
    unfiltered_channel_feed,
    unfiltered_state_entry,
    unfiltered_state_exit,
    final_valve_preactivation,
    increment_preactivation,
    summed_attenuation_both_ways,
    channel_fading_speed,
    channel_feed_filter,
    state_entry_filter,
    state_exit_filter,
    clustered_rescale_factor,
    final_projection_weights,
    specialist_rescale_factor,
    item_specialist_couple,
    selected_cluster_likelihood,
    selected_twin_scores_raw,
    specialist_gating_weights,
    specialist_raising_weights,
    specialist_lowering_weights,
):
    tokens_here = skip_stream_entering.shape[0]
    heads_here = increment_preactivation.shape[1]
    x_width = unfiltered_channel_feed.shape[1]
    b_width = unfiltered_state_entry.shape[1]
    groups_here = b_width // NS
    joined = jnp.concatenate(
        [unfiltered_channel_feed, unfiltered_state_entry, unfiltered_state_exit], axis=1
    )
    padded = extended(joined, ((SP, 0),), CONV // 2)
    kernel = jnp.concatenate([channel_feed_filter, state_entry_filter, state_exit_filter], axis=1)
    summed = jnp.zeros(joined.shape, jnp.float32)
    for offset in range(CONV):
        summed = summed + kernel[offset] * padded[offset : offset + tokens_here].astype(jnp.float32)
    conv_out = jax.nn.silu(summed).astype(jnp.bfloat16)
    x_conv = conv_out[:, :x_width].reshape(tokens_here, heads_here, HD)
    b_conv = conv_out[:, x_width : x_width + b_width].reshape(tokens_here, groups_here, NS)
    c_conv = conv_out[:, x_width + b_width :].reshape(tokens_here, groups_here, NS)
    whole_increment_list = jax.nn.softplus(increment_preactivation)
    whole_attenuation_list = (
        -whole_increment_list * channel_fading_speed[:, :, None] + summed_attenuation_both_ways
    )
    within, state_fwd, state_bwd, total_fwd, total_bwd, factor_fwd, factor_bwd, c_head = (
        block_parts(
            x_conv,
            b_conv,
            c_conv,
            whole_increment_list[0],
            whole_increment_list[1],
            whole_attenuation_list[0],
            whole_attenuation_list[1],
        )
    )
    empty = (jnp.zeros_like(total_fwd), jnp.zeros_like(state_fwd))
    incoming_fwd = carried_in((total_fwd, state_fwd), SP, compose, empty, False)[1]
    incoming_bwd = carried_in((total_bwd, state_bwd), SP, compose, empty, True)[1]
    mixer_out = (
        within
        + read_state(c_head, factor_fwd, incoming_fwd)
        + read_state(c_head, factor_bwd, incoming_bwd)
    )
    gated = mixer_out.reshape(tokens_here, x_width) * jax.nn.silu(
        final_valve_preactivation.astype(jnp.float32)
    )
    grouped = gated.reshape(tokens_here, groups_here, -1)
    grouped = grouped * lax.rsqrt(jnp.mean(grouped * grouped, axis=-1, keepdims=True) + group_eps)
    mixed = (grouped.reshape(tokens_here, x_width) * clustered_rescale_factor).astype(jnp.bfloat16)
    projected = jnp.dot(
        lax.all_gather(mixed, "tp", axis=1, tiled=True),
        final_projection_weights,
        preferred_element_type=jnp.float32,
    )
    stream = (skip_stream_entering.astype(jnp.float32) + projected).astype(jnp.bfloat16)
    stream_f = stream.astype(jnp.float32)
    col_count = skip_stream_entering.shape[1]
    whole_rows = lax.all_gather(stream, "tp", axis=1, tiled=True).astype(jnp.float32)
    normal_rows = (
        whole_rows
        * lax.rsqrt(jnp.mean(whole_rows * whole_rows, axis=-1, keepdims=True) + stream_eps)
        * specialist_rescale_factor
    ).astype(jnp.bfloat16)
    expert_total = lax.axis_size(SP)
    capacity = 4 * tokens_here // expert_total
    flat_ids = item_specialist_couple.reshape(-1)
    assignments = flat_ids.shape[0]
    expert_iota = lax.broadcasted_iota(jnp.int32, (assignments, expert_total), 1)
    one_hot = (flat_ids[:, None] == expert_iota).astype(jnp.int32)
    ranking = jnp.sum((jnp.cumsum(one_hot, axis=0) - 1) * one_hot, axis=1)
    slot_index = flat_ids * capacity + ranking
    slot_iota = lax.broadcasted_iota(jnp.int32, (expert_total * capacity, assignments), 0)
    selector = (slot_index[None, :] == slot_iota).astype(jnp.bfloat16)
    selector = jnp.sum(selector.reshape(expert_total * capacity, tokens_here, -1), axis=2)
    weight_gate = specialist_gating_weights[0]
    weight_up = specialist_raising_weights[0]
    weight_down = specialist_lowering_weights[0]
    outgoing = jnp.dot(selector, normal_rows, preferred_element_type=jnp.float32).astype(
        jnp.bfloat16
    )
    outgoing = outgoing.reshape(expert_total, capacity, D)
    arrived = lax.all_to_all(outgoing, SP, split_axis=0, concat_axis=0, tiled=True)
    sources = arrived.shape[0]
    slot_count = arrived.shape[1]
    rows = arrived.reshape(sources * slot_count, arrived.shape[2])
    gate = jnp.dot(rows, weight_gate, preferred_element_type=jnp.float32)
    upward = jnp.dot(rows, weight_up, preferred_element_type=jnp.float32)
    hidden = (jax.nn.silu(gate) * upward).astype(jnp.bfloat16)
    partial_out = jnp.dot(hidden, weight_down, preferred_element_type=jnp.float32).astype(
        jnp.bfloat16
    )
    partial_out = partial_out.reshape(sources, slot_count, partial_out.shape[1])
    expert_cols = sum_at_owner(partial_out, "tp", 2).astype(jnp.bfloat16)
    returned = lax.all_to_all(expert_cols, SP, split_axis=0, concat_axis=0, tiled=True)
    flat_back = returned.reshape(expert_total * capacity, col_count)
    picked = (
        jnp.take(flat_back, slot_index, axis=0)
        .astype(jnp.float32)
        .reshape(tokens_here, -1, col_count)
    )
    first = jax.nn.sigmoid(selected_twin_scores_raw[:, 0] - selected_twin_scores_raw[:, 1])
    route_weight = selected_cluster_likelihood[:, None] * jnp.stack([first, 1.0 - first], axis=1)
    experts_sum = jnp.sum(route_weight[:, :, None] * picked, axis=1)
    return (stream_f + experts_sum).astype(jnp.bfloat16)


def solution(mesh):
    torus = Mesh(mesh.devices.reshape(8, 4, mesh.shape["tp"]), ("sp_0", "sp_1", "tp"))
    return jax.shard_map(
        body,
        mesh=torus,
        in_specs=(
            P(SP, "tp"),
            P(SP, "tp"),
            P(SP, "tp"),
            P(SP, "tp"),
            P(SP, "tp"),
            P(None, "tp", SP),
            P(None, "tp", SP),
            P(None, "tp"),
            P(None, "tp"),
            P(None, "tp"),
            P(None, "tp"),
            P("tp"),
            P(None, "tp"),
            P(),
            P(SP, None),
            P(SP),
            P(SP, None),
            P(SP, None, "tp"),
            P(SP, None, "tp"),
            P(SP, "tp", None),
        ),
        out_specs=P(SP, "tp"),
        check_vma=False,
    )
```

profile of v0, /device:TPU:1, one launch (start us, length us, event | category | flops | bytes accessed | tf_op | source)
XLA Modules:
  0.0 280.2 jit_solution(5651927392031734438)
XLA Ops:
  0.0 0.9 constant_dynamic-update-slice_fusion.5
  0.9 0.8 constant_dynamic-update-slice_fusion.4
  1.6 0.8 constant_dynamic-update-slice_fusion.3
  2.4 3.9 %collective-permute-start = (bf16[2,384]{1,0:T(2,128)(2,1)S(1)}, bf16[2,384]{1,0:T(2,128)(2,1)S(1)}, u32[]{:S(2)}, u32[]{:S(2)}) collective-permute-start(bf16[2,384]{1,0:T(2,128)(2,1)S(1)} %get-tuple-element.47), channel_id=1, source_target_pairs={{0,16},{16,32},{32,48},{48,64},{64,80},{80,96},{96,112},{112,128},... | collective-permute-start | bytes 4616 | tf_op jit(solution)/shard_map/ppermute | solution.py:25
  6.3 1.3 collective-permute-start.1
  7.7 0.8 copy.71
  8.8 0.8 multiply_add_fusion
  10.7 0.7 constant_dynamic-update-slice_fusion.2
  11.4 0.7 constant_dynamic-update-slice_fusion.1
  12.1 0.7 constant_dynamic-update-slice_fusion
  12.8 0.6 reduce-window.6
  14.0 0.7 compare_and_fusion
  15.4 10.4 %all-gather.6 = bf16[4,129,128]{2,1,0:T(8,128)(2,1)S(1)} all-gather(bf16[1,129,128]{2,1,0:T(8,128)(2,1)S(1)} %maximum_bitcast_fusion.2), channel_id=4, replica_groups=mesh['sp_0'=8,'sp_1'=4,'tp'=16] {'sp_1'}, dimensions={0}, use_global_device_ids=true | all-gather | bytes 165120 | tf_op jit(solution)/shard_map/all_gather | solution.py:48
  26.6 27.4 %all-gather.7 = bf16[8,129,128]{2,1,0:T(8,128)(2,1)S(1)} all-gather(bf16[1,129,128]{2,1,0:T(8,128)(2,1)S(1)} %maximum_bitcast_fusion.3), channel_id=5, replica_groups=mesh['sp_0'=8,'sp_1'=4,'tp'=16] {'sp_0'}, dimensions={0}, use_global_device_ids=true | all-gather | bytes 297216 | tf_op jit(solution)/shard_map/all_gather | solution.py:48
  54.2 9.1 %all-gather.4 = bf16[4,129,128]{2,1,0:T(8,128)(2,1)S(1)} all-gather(bf16[1,129,128]{2,1,0:T(8,128)(2,1)S(1)} %maximum_bitcast_fusion), channel_id=2, replica_groups=mesh['sp_0'=8,'sp_1'=4,'tp'=16] {'sp_1'}, dimensions={0}, use_global_device_ids=true | all-gather | bytes 165120 | tf_op jit(solution)/shard_map/all_gather | solution.py:48
  64.2 18.5 %all-gather.5 = bf16[8,129,128]{2,1,0:T(8,128)(2,1)S(1)} all-gather(bf16[1,129,128]{2,1,0:T(8,128)(2,1)S(1)} %maximum_bitcast_fusion.1), channel_id=3, replica_groups=mesh['sp_0'=8,'sp_1'=4,'tp'=16] {'sp_0'}, dimensions={0}, use_global_device_ids=true | all-gather | bytes 297216 | tf_op jit(solution)/shard_map/all_gather | solution.py:48
  83.4 0.5 fusion.5
  84.8 37.9 %all_gather.38 = bf16[128,2048]{1,0:T(8,128)(2,1)S(1)} all-gather(bf16[128,128]{1,0:T(8,128)(2,1)S(1)} %multiply_convert_fusion.1), channel_id=1, replica_groups=mesh['sp_0'=8,'sp_1'=4,'tp'=16] {'tp'}, dimensions={1}, use_global_device_ids=true | all-gather | bytes 557056 | tf_op jit(solution)/shard_map/all_gather | solution.py:213
  123.0 16.4 %all_gather.39 = bf16[128,2048]{1,0:T(8,128)(2,1)S(1)} all-gather(bf16[128,128]{1,0:T(8,128)(2,1)S(1)} %fusion.6), channel_id=1, replica_groups=mesh['sp_0'=8,'sp_1'=4,'tp'=16] {'tp'}, dimensions={1}, use_global_device_ids=true | all-gather | bytes 557056 | tf_op jit(solution)/shard_map/all_gather | solution.py:220
  139.6 0.8 convolution_convert_fusion.1
  140.4 55.6 %all_to_all.15 = bf16[32,16,2048]{2,1,0:T(8,128)(2,1)S(1)} all-to-all(bf16[32,16,2048]{2,1,0:T(8,128)(2,1)S(1)} %bitcast.252), channel_id=1, replica_groups=mesh['sp_0'=8,'sp_1'=4,'tp'=16] {'sp_0','sp_1'}, dimensions={0} | all-to-all | bytes 4194304 | tf_op jit(solution)/shard_map/all_to_all | solution.py:244
  196.0 1.5 fusion.12
  197.5 5.0 %fusion = bf16[64,8,16,128]{3,1,2,0:T(8,128)(2,1)} fusion(bf16[1,256,2048]{2,1,0:T(8,128)(2,1)S(1)} %copy-done, bf16[512,2048]{1,0:T(8,128)(2,1)S(1)} %bitcast.256, bf16[1,2048,256]{2,1,0:T(8,128)(2,1)} %param.38, f32[512,256]{1,0:T(8,128)} %fusion.12), kind=kOutput, calls=%fused_computation.4 | convolution fusion | flops 1075576832 | bytes 6815744 | tf_op jit(solution)/shard_map/dot_general | solution.py:251
  202.6 2.2 copy.83
  204.8 1.9 copy.90
  206.7 6.9 %all-to-all-start.1 = ((bf16[16,32,16,128]{3,2,1,0:T(8,128)(2,1)}), bf16[16,32,16,128]{3,2,1,0:T(8,128)(2,1)S(1)}, u32[]{:S(2)}, u32[]{:S(2)}) async-start(bf16[16,32,16,128]{3,2,1,0:T(8,128)(2,1)} %bitcast.251), calls=%async_computation.1 | async-start | bytes 4194304 | tf_op jit(solution)/shard_map/all_to_all | solution.py:87
  214.2 48.5 %all-to-all-done.1 = bf16[16,32,16,128]{3,2,1,0:T(8,128)(2,1)S(1)} async-done(((bf16[16,32,16,128]{3,2,1,0:T(8,128)(2,1)}), bf16[16,32,16,128]{3,2,1,0:T(8,128)(2,1)S(1)}, u32[]{:S(2)}, u32[]{:S(2)}) %all-to-all-start.1) | async-done | bytes 2097184 | tf_op jit(solution)/shard_map/all_to_all | solution.py:87
  262.6 0.9 reduce_sum.69
  263.6 5.3 %all-to-all-start.2 = ((bf16[32,16,128]{2,1,0:T(8,128)(2,1)}), bf16[32,16,128]{2,1,0:T(8,128)(2,1)S(1)}, u32[]{:S(2)}, u32[]{:S(2)}) async-start(bf16[32,16,128]{2,1,0:T(8,128)(2,1)} %reduce_sum.69), calls=%async_computation.2 | async-start | bytes 262144 | tf_op jit(solution)/shard_map/all_to_all | solution.py:256
  268.9 9.4 %all-to-all-done.2 = bf16[32,16,128]{2,1,0:T(8,128)(2,1)S(1)} async-done(((bf16[32,16,128]{2,1,0:T(8,128)(2,1)}), bf16[32,16,128]{2,1,0:T(8,128)(2,1)S(1)}, u32[]{:S(2)}, u32[]{:S(2)}) %all-to-all-start.2) | async-done | bytes 131104 | tf_op jit(solution)/shard_map/all_to_all | solution.py:256
  278.3 0.9 gather_fusion
  279.6 0.6 add_convert_fusion
  (114 shorter events, 7.3 us)
Async XLA Ops:
  0.0 197.5 %copy-start = (bf16[1,256,2048]{2,1,0:T(8,128)(2,1)S(1)}, bf16[1,256,2048]{2,1,0:T(8,128)(2,1)}, u32[]{:S(2)}) copy-start(bf16[1,256,2048]{2,1,0:T(8,128)(2,1)} %param.39) | copy-start | bytes 3145732
  2.4 12.4 %collective-permute-start = (bf16[2,384]{1,0:T(2,128)(2,1)S(1)}, bf16[2,384]{1,0:T(2,128)(2,1)S(1)}, u32[]{:S(2)}, u32[]{:S(2)}) collective-permute-start(bf16[2,384]{1,0:T(2,128)(2,1)S(1)} %get-tuple-element.47), channel_id=1, source_target_pairs={{0,16},{16,32},{32,48},{48,64},{64,80},{80,96},{96,112},{112,128},... | collective-permute-start | bytes 4616 | tf_op jit(solution)/shard_map/ppermute | solution.py:25
  6.3 8.4 %collective-permute-start.1 = (bf16[2,384]{1,0:T(2,128)(2,1)S(1)}, bf16[2,384]{1,0:T(2,128)(2,1)S(1)}, u32[]{:S(2)}, u32[]{:S(2)}) collective-permute-start(bf16[2,384]{1,0:T(2,128)(2,1)S(1)} %get-tuple-element.48), channel_id=1, source_target_pairs={{16,0},{32,16},{48,32},{64,48},{80,64},{96,80},{112,96},{128,112},... | collective-permute-start | bytes 4616 | tf_op jit(solution)/shard_map/ppermute | solution.py:27
  82.7 1.9 copy-start.2
  82.7 2.0 copy-start.7
  82.7 40.0 %copy-start.1 = (bf16[2048,128]{1,0:T(8,128)(2,1)S(1)}, bf16[2048,128]{1,0:T(8,128)(2,1)}, u32[]{:S(2)}) copy-start(bf16[2048,128]{1,0:T(8,128)(2,1)} %param.32) | copy-start | bytes 1572868
  82.7 40.0 %copy-start.3 = (bf16[128,128]{1,0:T(8,128)(2,1)S(1)}, bf16[128,128]{1,0:T(8,128)(2,1)}, u32[]{:S(2)}) copy-start(bf16[128,128]{1,0:T(8,128)(2,1)} %param.20) | copy-start | bytes 98308
  83.9 55.7 %copy-start.5 = (f32[2048]{0:T(1024)S(1)}, f32[2048]{0:T(1024)}, u32[]{:S(2)}) copy-start(f32[2048]{0:T(1024)} %param.33) | copy-start | bytes 24580
  140.4 55.6 %copy-start.9 = (bf16[1,2048,256]{2,1,0:T(8,128)(2,1)S(1)}, bf16[1,2048,256]{2,1,0:T(8,128)(2,1)}, u32[]{:S(2)}) copy-start(bf16[1,2048,256]{2,1,0:T(8,128)(2,1)} %param.37) | copy-start | bytes 3145732
  206.7 6.9 %copy-start.4 = (s32[128,2]{0,1:T(2,128)S(1)}, s32[128,2]{0,1:T(2,128)}, u32[]{:S(2)}) copy-start(s32[128,2]{0,1:T(2,128)} %param.34) | copy-start | bytes 3076
  206.7 7.3 %copy-start.6 = (f32[128,2]{0,1:T(2,128)S(1)}, f32[128,2]{0,1:T(2,128)}, u32[]{:S(2)}) copy-start(f32[128,2]{0,1:T(2,128)} %param.36) | copy-start | bytes 3076
  206.7 7.4 %copy-start.8 = (f32[128]{0:T(128)S(1)}, f32[128]{0:T(128)}, u32[]{:S(2)}) copy-start(f32[128]{0:T(128)} %param.35) | copy-start | bytes 1540
  206.7 56.0 %all-to-all-start.1 = ((bf16[16,32,16,128]{3,2,1,0:T(8,128)(2,1)}), bf16[16,32,16,128]{3,2,1,0:T(8,128)(2,1)S(1)}, u32[]{:S(2)}, u32[]{:S(2)}) async-start(bf16[16,32,16,128]{3,2,1,0:T(8,128)(2,1)} %bitcast.251), calls=%async_computation.1 | async-start | bytes 4194304 | tf_op jit(solution)/shard_map/all_to_all | solution.py:87
  263.6 14.8 %all-to-all-start.2 = ((bf16[32,16,128]{2,1,0:T(8,128)(2,1)}), bf16[32,16,128]{2,1,0:T(8,128)(2,1)S(1)}, u32[]{:S(2)}, u32[]{:S(2)}) async-start(bf16[32,16,128]{2,1,0:T(8,128)(2,1)} %reduce_sum.69), calls=%async_computation.2 | async-start | bytes 262144 | tf_op jit(solution)/shard_map/all_to_all | solution.py:256
where the time goes:
time: 281 us; the launch traced here: 280 us
  blocking collectives  175 us (62%)
  waiting for transfers between devices  57.9 us (21%)
  starting transfers between devices  17.4 us (6%)
  local copies, waits for them, and re-layouts  13.4 us (5%)
  matrix products  9.61 us (3%)
  other arithmetic  6.01 us (2%)
    all_gather x4, blocking collectives, all_in_one(): both, at, found = (lax.all_gather(jnp.concatenate(lines), axis), 0, {})  65.3 us
    all_to_all x1, blocking collectives, body(): lax.all_to_all(outgoing, SP, split_axis=0, concat_axis=0, tiled=True)  55.6 us
    all_to_all x1, waiting for transfers between devices, sum_at_owner(): parts = lax.all_to_all(in_blocks(shard, dim, peers), axis, 0, 0, tiled=True)  48.5 us
    all_gather x1, blocking collectives, body(): lax.all_gather(mixed, 'tp', axis=1, tiled=True)  37.9 us
    all_gather x1, blocking collectives, body(): lax.all_gather(stream, 'tp', axis=1, tiled=True).astype(jnp.float32)  16.4 us
    all_to_all x1, waiting for transfers between devices, body(): lax.all_to_all(expert_cols, SP, split_axis=0, concat_axis=0, tiled=True)  9.43 us
    all_to_all x1, starting transfers between devices, sum_at_owner(): parts = lax.all_to_all(in_blocks(shard, dim, peers), axis, 0, 0, tiled=True)  6.91 us
    unnamed x30, local copies, waits for them, and re-layouts  6.06 us
  transfers between devices with their start and end apart: 4, of which 2 were waited for; matrix products, arithmetic and copies ran while one was open for 3% of the time, Pallas kernels for 0%

commit v1 on v0

--- a/solution.py
+++ b/solution.py
@@ -12,6 +12,12 @@
 HIGHEST = lax.Precision.HIGHEST
 group_eps = 1e-05
 stream_eps = 1e-06
+
+
+def gather_from_all(x, axis, dim):
+    peers = lax.axis_size(axis)
+    repeats = [peers if d == dim else 1 for d in range(x.ndim)]
+    return lax.all_to_all(jnp.tile(x, repeats), axis, split_axis=dim, concat_axis=dim, tiled=True)
 
 
 def extended(cells, sides, width):
@@ -210,7 +216,7 @@
     grouped = grouped * lax.rsqrt(jnp.mean(grouped * grouped, axis=-1, keepdims=True) + group_eps)
     mixed = (grouped.reshape(tokens_here, x_width) * clustered_rescale_factor).astype(jnp.bfloat16)
     projected = jnp.dot(
-        lax.all_gather(mixed, "tp", axis=1, tiled=True),
+        gather_from_all(mixed, "tp", 1),
         final_projection_weights,
         preferred_element_type=jnp.float32,
     )

time: 281 us -> 284 us (1.011)
  blocking collectives: 175 us -> 137 us
  starting transfers between devices: 17.4 us -> 43.4 us
  waiting for transfers between devices: 57.9 us -> 73.5 us
    all_gather x1 -> x0, blocking collectives: 37.9 us -> none  [body(): lax.all_gather(mixed, 'tp', axis=1, tiled=True)]
    all_to_all x0 -> x1, starting transfers between devices: none -> 25.8 us  [gather_from_all(): lax.all_to_all(jnp.tile(x, repeats), axis, split_axis=dim, concat_axis=di...]
    all_to_all x0 -> x1, waiting for transfers between devices: none -> 15.5 us  [gather_from_all(): lax.all_to_all(jnp.tile(x, repeats), axis, split_axis=dim, concat_axis=di...]
  transfers between devices with their start and end apart: 4 -> 5, of which waited for: 2 -> 3; matrix products, arithmetic and copies ran while one was open for 3% -> 2% of each run, Pallas kernels for 0% -> 0%
where the time goes in v1:
time: 284 us
  blocking collectives  137 us (48%)
  waiting for transfers between devices  73.5 us (26%)
  starting transfers between devices  43.4 us (15%)
  local copies, waits for them, and re-layouts  13.9 us (5%)
  matrix products  9.69 us (3%)
  other arithmetic  5.32 us (2%)
    all_gather x4, blocking collectives, all_in_one(): both, at, found = (lax.all_gather(jnp.concatenate(lines), axis), 0, {})  65.6 us
    all_to_all x1, blocking collectives, body(): lax.all_to_all(outgoing, SP, split_axis=0, concat_axis=0, tiled=True)  55.7 us
    all_to_all x1, waiting for transfers between devices, sum_at_owner(): parts = lax.all_to_all(in_blocks(shard, dim, peers), axis, 0, 0, tiled=True)  48.5 us
    all_to_all x1, starting transfers between devices, gather_from_all(): lax.all_to_all(jnp.tile(x, repeats), axis, split_axis=dim, concat_axis=di...  25.8 us
    all_gather x1, blocking collectives, body(): lax.all_gather(stream, 'tp', axis=1, tiled=True).astype(jnp.float32)  15.9 us
    all_to_all x1, waiting for transfers between devices, gather_from_all(): lax.all_to_all(jnp.tile(x, repeats), axis, split_axis=dim, concat_axis=di...  15.5 us
    all_to_all x1, waiting for transfers between devices, body(): lax.all_to_all(expert_cols, SP, split_axis=0, concat_axis=0, tiled=True)  9.43 us
    all_to_all x1, starting transfers between devices, sum_at_owner(): parts = lax.all_to_all(in_blocks(shard, dim, peers), axis, 0, 0, tiled=True)  7.09 us
  transfers between devices with their start and end apart: 5, of which 3 were waited for; matrix products, arithmetic and copies ran while one was open for 2% of the time, Pallas kernels for 0%

profile of v1, /device:TPU:1, one launch (start us, length us, event | category | flops | bytes accessed | tf_op | source)
XLA Modules:
  0.0 283.6 jit_solution(14853893391327299424)
XLA Ops:
  0.0 0.9 constant_dynamic-update-slice_fusion.5
  0.9 0.8 constant_dynamic-update-slice_fusion.4
  1.6 0.8 constant_dynamic-update-slice_fusion.3
  2.4 3.9 %collective-permute-start = (bf16[2,384]{1,0:T(2,128)(2,1)S(1)}, bf16[2,384]{1,0:T(2,128)(2,1)S(1)}, u32[]{:S(2)}, u32[]{:S(2)}) collective-permute-start(bf16[2,384]{1,0:T(2,128)(2,1)S(1)} %get-tuple-element.47), channel_id=1, source_target_pairs={{0,16},{16,32},{32,48},{48,64},{64,80},{80,96},{96,112},{112,128},... | collective-permute-start | bytes 4616 | tf_op jit(solution)/shard_map/ppermute | solution.py:31
  6.3 1.3 collective-permute-start.1
  7.7 0.8 multiply_add_fusion
  9.6 0.7 constant_dynamic-update-slice_fusion.2
  10.3 0.7 constant_dynamic-update-slice_fusion.1
  11.0 0.7 constant_dynamic-update-slice_fusion
  12.4 10.7 %all-gather.6 = bf16[4,129,128]{2,1,0:T(8,128)(2,1)S(1)} all-gather(bf16[1,129,128]{2,1,0:T(8,128)(2,1)S(1)} %maximum_bitcast_fusion.2), channel_id=4, replica_groups=mesh['sp_0'=8,'sp_1'=4,'tp'=16] {'sp_1'}, dimensions={0}, use_global_device_ids=true | all-gather | bytes 165120 | tf_op jit(solution)/shard_map/all_gather | solution.py:54
  23.9 27.0 %all-gather.7 = bf16[8,129,128]{2,1,0:T(8,128)(2,1)S(1)} all-gather(bf16[1,129,128]{2,1,0:T(8,128)(2,1)S(1)} %maximum_bitcast_fusion.3), channel_id=5, replica_groups=mesh['sp_0'=8,'sp_1'=4,'tp'=16] {'sp_0'}, dimensions={0}, use_global_device_ids=true | all-gather | bytes 297216 | tf_op jit(solution)/shard_map/all_gather | solution.py:54
  51.2 9.1 %all-gather.4 = bf16[4,129,128]{2,1,0:T(8,128)(2,1)S(1)} all-gather(bf16[1,129,128]{2,1,0:T(8,128)(2,1)S(1)} %maximum_bitcast_fusion), channel_id=2, replica_groups=mesh['sp_0'=8,'sp_1'=4,'tp'=16] {'sp_1'}, dimensions={0}, use_global_device_ids=true | all-gather | bytes 165120 | tf_op jit(solution)/shard_map/all_gather | solution.py:54
  61.2 18.8 %all-gather.5 = bf16[8,129,128]{2,1,0:T(8,128)(2,1)S(1)} all-gather(bf16[1,129,128]{2,1,0:T(8,128)(2,1)S(1)} %maximum_bitcast_fusion.1), channel_id=3, replica_groups=mesh['sp_0'=8,'sp_1'=4,'tp'=16] {'sp_0'}, dimensions={0}, use_global_device_ids=true | all-gather | bytes 297216 | tf_op jit(solution)/shard_map/all_gather | solution.py:54
  80.7 0.5 fusion.5
  82.1 0.9 tile.2
  83.0 25.8 %all-to-all-start = ((bf16[128,16,128]{2,0,1:T(8,128)(2,1)}), bf16[128,16,128]{2,0,1:T(8,128)(2,1)S(1)}, u32[]{:S(2)}, u32[]{:S(2)}) async-start(bf16[128,16,128]{2,0,1:T(8,128)(2,1)} %tile.2), calls=%async_computation | async-start | bytes 1048576 | tf_op jit(solution)/shard_map/all_to_all | solution.py:20
  109.2 0.6 reduce-window.6
  110.5 15.5 %all-to-all-done = bf16[128,16,128]{2,0,1:T(8,128)(2,1)S(1)} async-done(((bf16[128,16,128]{2,0,1:T(8,128)(2,1)}), bf16[128,16,128]{2,0,1:T(8,128)(2,1)S(1)}, u32[]{:S(2)}, u32[]{:S(2)}) %all-to-all-start) | async-done | bytes 524320 | tf_op jit(solution)/shard_map/all_to_all | solution.py:20
  126.7 15.9 %all_gather.35 = bf16[128,2048]{1,0:T(8,128)(2,1)S(1)} all-gather(bf16[128,128]{1,0:T(8,128)(2,1)S(1)} %fusion.6), channel_id=1, replica_groups=mesh['sp_0'=8,'sp_1'=4,'tp'=16] {'tp'}, dimensions={1}, use_global_device_ids=true | all-gather | bytes 557056 | tf_op jit(solution)/shard_map/all_gather | solution.py:226
  142.8 0.8 convolution_convert_fusion.1
  143.6 55.7 %all_to_all.24 = bf16[32,16,2048]{2,1,0:T(8,128)(2,1)S(1)} all-to-all(bf16[32,16,2048]{2,1,0:T(8,128)(2,1)S(1)} %bitcast.253), channel_id=1, replica_groups=mesh['sp_0'=8,'sp_1'=4,'tp'=16] {'sp_0','sp_1'}, dimensions={0} | all-to-all | bytes 4194304 | tf_op jit(solution)/shard_map/all_to_all | solution.py:250
  199.3 1.5 fusion.12
  200.8 5.0 %fusion = bf16[64,8,16,128]{3,1,2,0:T(8,128)(2,1)} fusion(bf16[1,256,2048]{2,1,0:T(8,128)(2,1)S(1)} %copy-done, bf16[512,2048]{1,0:T(8,128)(2,1)S(1)} %bitcast.257, bf16[1,2048,256]{2,1,0:T(8,128)(2,1)} %param.38, f32[512,256]{1,0:T(8,128)} %fusion.12), kind=kOutput, calls=%fused_computation.4 | convolution fusion | flops 1075576832 | bytes 6815744 | tf_op jit(solution)/shard_map/dot_general | solution.py:257
  205.8 2.2 copy.96
  208.0 1.9 copy.103
  209.9 7.1 %all-to-all-start.2 = ((bf16[16,32,16,128]{3,2,1,0:T(8,128)(2,1)}), bf16[16,32,16,128]{3,2,1,0:T(8,128)(2,1)S(1)}, u32[]{:S(2)}, u32[]{:S(2)}) async-start(bf16[16,32,16,128]{3,2,1,0:T(8,128)(2,1)} %bitcast.252), calls=%async_computation.2 | async-start | bytes 4194304 | tf_op jit(solution)/shard_map/all_to_all | solution.py:93
  217.6 48.5 %all-to-all-done.2 = bf16[16,32,16,128]{3,2,1,0:T(8,128)(2,1)S(1)} async-done(((bf16[16,32,16,128]{3,2,1,0:T(8,128)(2,1)}), bf16[16,32,16,128]{3,2,1,0:T(8,128)(2,1)S(1)}, u32[]{:S(2)}, u32[]{:S(2)}) %all-to-all-start.2) | async-done | bytes 2097184 | tf_op jit(solution)/shard_map/all_to_all | solution.py:93
  266.1 0.9 reduce_sum.69
  267.0 5.3 %all-to-all-start.3 = ((bf16[32,16,128]{2,1,0:T(8,128)(2,1)}), bf16[32,16,128]{2,1,0:T(8,128)(2,1)S(1)}, u32[]{:S(2)}, u32[]{:S(2)}) async-start(bf16[32,16,128]{2,1,0:T(8,128)(2,1)} %reduce_sum.69), calls=%async_computation.3 | async-start | bytes 262144 | tf_op jit(solution)/shard_map/all_to_all | solution.py:262
  272.4 9.4 %all-to-all-done.3 = bf16[32,16,128]{2,1,0:T(8,128)(2,1)S(1)} async-done(((bf16[32,16,128]{2,1,0:T(8,128)(2,1)}), bf16[32,16,128]{2,1,0:T(8,128)(2,1)S(1)}, u32[]{:S(2)}, u32[]{:S(2)}) %all-to-all-start.3) | async-done | bytes 131104 | tf_op jit(solution)/shard_map/all_to_all | solution.py:262
  281.8 0.9 gather_fusion
  283.0 0.6 add_convert_fusion
  (117 shorter events, 7.8 us)
Async XLA Ops:
  0.0 200.8 %copy-start = (bf16[1,256,2048]{2,1,0:T(8,128)(2,1)S(1)}, bf16[1,256,2048]{2,1,0:T(8,128)(2,1)}, u32[]{:S(2)}) copy-start(bf16[1,256,2048]{2,1,0:T(8,128)(2,1)} %param.39) | copy-start | bytes 3145732
  2.4 9.4 %collective-permute-start = (bf16[2,384]{1,0:T(2,128)(2,1)S(1)}, bf16[2,384]{1,0:T(2,128)(2,1)S(1)}, u32[]{:S(2)}, u32[]{:S(2)}) collective-permute-start(bf16[2,384]{1,0:T(2,128)(2,1)S(1)} %get-tuple-element.47), channel_id=1, source_target_pairs={{0,16},{16,32},{32,48},{48,64},{64,80},{80,96},{96,112},{112,128},... | collective-permute-start | bytes 4616 | tf_op jit(solution)/shard_map/ppermute | solution.py:31
  6.3 5.5 %collective-permute-start.1 = (bf16[2,384]{1,0:T(2,128)(2,1)S(1)}, bf16[2,384]{1,0:T(2,128)(2,1)S(1)}, u32[]{:S(2)}, u32[]{:S(2)}) collective-permute-start(bf16[2,384]{1,0:T(2,128)(2,1)S(1)} %get-tuple-element.48), channel_id=1, source_target_pairs={{16,0},{32,16},{48,32},{64,48},{80,64},{96,80},{112,96},{128,112},... | collective-permute-start | bytes 4616 | tf_op jit(solution)/shard_map/ppermute | solution.py:33
  80.0 1.9 copy-start.2
  80.0 2.0 copy-start.7
  80.7 28.1 %copy-start.4 = (s32[128,2]{0,1:T(2,128)S(1)}, s32[128,2]{0,1:T(2,128)}, u32[]{:S(2)}) copy-start(s32[128,2]{0,1:T(2,128)} %param.34) | copy-start | bytes 3076
  81.2 45.1 %copy-start.1 = (bf16[2048,128]{1,0:T(8,128)(2,1)S(1)}, bf16[2048,128]{1,0:T(8,128)(2,1)}, u32[]{:S(2)}) copy-start(bf16[2048,128]{1,0:T(8,128)(2,1)} %param.32) | copy-start | bytes 1572868
  81.2 45.1 %copy-start.3 = (bf16[128,128]{1,0:T(8,128)(2,1)S(1)}, bf16[128,128]{1,0:T(8,128)(2,1)}, u32[]{:S(2)}) copy-start(bf16[128,128]{1,0:T(8,128)(2,1)} %param.20) | copy-start | bytes 98308
  83.0 43.0 %all-to-all-start = ((bf16[128,16,128]{2,0,1:T(8,128)(2,1)}), bf16[128,16,128]{2,0,1:T(8,128)(2,1)S(1)}, u32[]{:S(2)}, u32[]{:S(2)}) async-start(bf16[128,16,128]{2,0,1:T(8,128)(2,1)} %tile.2), calls=%async_computation | async-start | bytes 1048576 | tf_op jit(solution)/shard_map/all_to_all | solution.py:20
  108.8 34.0 %copy-start.5 = (f32[2048]{0:T(1024)S(1)}, f32[2048]{0:T(1024)}, u32[]{:S(2)}) copy-start(f32[2048]{0:T(1024)} %param.33) | copy-start | bytes 24580
  143.6 55.7 %copy-start.9 = (bf16[1,2048,256]{2,1,0:T(8,128)(2,1)S(1)}, bf16[1,2048,256]{2,1,0:T(8,128)(2,1)}, u32[]{:S(2)}) copy-start(bf16[1,2048,256]{2,1,0:T(8,128)(2,1)} %param.37) | copy-start | bytes 3145732
  209.9 7.5 %copy-start.6 = (f32[128,2]{0,1:T(2,128)S(1)}, f32[128,2]{0,1:T(2,128)}, u32[]{:S(2)}) copy-start(f32[128,2]{0,1:T(2,128)} %param.36) | copy-start | bytes 3076
  209.9 7.5 %copy-start.8 = (f32[128]{0:T(128)S(1)}, f32[128]{0:T(128)}, u32[]{:S(2)}) copy-start(f32[128]{0:T(128)} %param.35) | copy-start | bytes 1540
  209.9 56.1 %all-to-all-start.2 = ((bf16[16,32,16,128]{3,2,1,0:T(8,128)(2,1)}), bf16[16,32,16,128]{3,2,1,0:T(8,128)(2,1)S(1)}, u32[]{:S(2)}, u32[]{:S(2)}) async-start(bf16[16,32,16,128]{3,2,1,0:T(8,128)(2,1)} %bitcast.252), calls=%async_computation.2 | async-start | bytes 4194304 | tf_op jit(solution)/shard_map/all_to_all | solution.py:93
  267.0 14.8 %all-to-all-start.3 = ((bf16[32,16,128]{2,1,0:T(8,128)(2,1)}), bf16[32,16,128]{2,1,0:T(8,128)(2,1)S(1)}, u32[]{:S(2)}, u32[]{:S(2)}) async-start(bf16[32,16,128]{2,1,0:T(8,128)(2,1)} %reduce_sum.69), calls=%async_computation.3 | async-start | bytes 262144 | tf_op jit(solution)/shard_map/all_to_all | solution.py:262
